TPU v7x, 32 devices: a whole 2x2x4 slice. The times are simulated.
32 devices in a mesh: ep: 8 (over z, y), tp: 4 (over x, core).
Axes of the slice: x: 2, y: 2, z: 4, core: 2. Of those that a mesh axis runs over, the one named last changes fastest.
Arguments:
- queries: bfloat16 [8192, 1024], P('ep', 'tp'), may hold values from -6 to 6
- keys: bfloat16 [8192, 1024], P('ep', 'tp'), may hold values from -6 to 6
- values: bfloat16 [8192, 2048], P('ep', 'tp'), may hold values from -6 to 6
- log_input_gate: float32 [8192, 8], P('ep', 'tp'), may hold values from -6 to 103
- forget_preactivation: float32 [8192, 8], P('ep', 'tp'), may hold values from 0 to 16
- forget_offset: float32 [8192, 8], P('ep', 'tp'), may hold values from -0.7 to 0
- head_norm_scale: float32 [2048], P('tp'), may hold values from 0.1 to 1.9
- memory_output_weight: bfloat16 [2048, 4096], P('tp'), may hold values from -0.125 to 0.125
- second_micro_tokens: bfloat16 [4096, 4096], P('ep'), may hold values from -6 to 6
- expert_norm_scale: float32 [4096], replicated, may hold values from 0.1 to 1.9
- expert_choice_index: int32 [4096, 2], P('ep'), may hold values from 0 to 15, all different within a row; in each aligned block of 512 rows (0 to 511, 512 to 1023, ...) at most 96 rows name the same one
- group_likelihood: float32 [4096], P('ep'), may hold values from 0.2 to 1
- expert_raw_weight: float32 [4096, 2], P('ep'), may hold values from 0.1 to 1
- gate_weight: bfloat16 [16, 4096, 1024], P('ep', None, 'tp'), may hold values from -0.09375 to 0.09375
- up_weight: bfloat16 [16, 4096, 1024], P('ep', None, 'tp'), may hold values from -0.09375 to 0.09375
- down_weight: bfloat16 [16, 1024, 4096], P('ep', 'tp'), may hold values from -0.1875 to 0.1875
Outputs:
- mixed: bfloat16 [8192, 4096], P(('ep', 'tp'))
- routed: bfloat16 [4096, 4096], P('ep', 'tp')
Inputs may be any that keep to these rules, and one draw needn't show every extreme that they name: `expert_choice_index`: each row names 2 different experts. Within the 512 rows of one index of ep (aligned blocks) no expert is named more than 96 times, and in some blocks one expert is named exactly 96 times.
All inputs are finite; a program needn't handle non-finite values.
Results may differ from a plain program's by a relative error of at most 0.012.
Values may be sent and summed in bfloat16 or wider, within the bound.
A program may use at most 192 MiB of HBM per device.

v0:
```python
import math
import jax
import jax.numpy as jnp
from jax import lax
from jax.sharding import PartitionSpec as P

BLOCK = 128
EPSILON = 1e-06
FLOOR_LOG = -1e30


def carried_in(value, axis, join, neutral):
    count, mine = (lax.axis_size(axis), lax.axis_index(axis))
    pieces = jax.tree.map(lambda part: lax.all_gather(part, axis), value)
    subtotal = jax.tree.map(
        lambda part, zero: jnp.full_like(part, 0) + jnp.asarray(zero, part.dtype), value, neutral
    )

    def turn(position, subtotal):
        longer = join(subtotal, jax.tree.map(lambda part: part[position], pieces))
        return jax.tree.map(lambda new, old: jnp.where(position < mine, new, old), longer, subtotal)

    return lax.fori_loop(0, count - 1, turn, subtotal)


def merge_states(earlier, later):
    memory_one, stable_one, total_one = earlier
    memory_two, stable_two, total_two = later
    highest = jnp.maximum(total_two + stable_one, stable_two)
    weight_one = jnp.exp(total_two + stable_one - highest)
    weight_two = jnp.exp(stable_two - highest)
    memory = weight_one[..., None, None] * memory_one + weight_two[..., None, None] * memory_two
    return (memory, highest, total_one + total_two)


def advance(carry, piece):
    return (merge_states(carry, piece), carry)


def recurrence_portion(
    queries,
    keys,
    values,
    log_input_gate,
    forget_preactivation,
    forget_offset,
    head_norm_scale,
    memory_output_weight,
):
    row_count, head_count = log_input_gate.shape
    key_width = queries.shape[1] // head_count
    value_width = values.shape[1] // head_count
    block_count = row_count // BLOCK
    qk_scale = 1.0 / math.sqrt(key_width)
    query_blocks = queries.reshape(block_count, BLOCK, head_count, key_width)
    key_blocks = keys.reshape(block_count, BLOCK, head_count, key_width)
    value_blocks = values.reshape(block_count, BLOCK, head_count, value_width)
    key_float = key_blocks.astype(jnp.float32) * qk_scale
    forget_log_factor = jax.nn.log_sigmoid(forget_preactivation) + forget_offset
    forget_log_factor = forget_log_factor.reshape(block_count, BLOCK, head_count).transpose(0, 2, 1)
    in_gate = log_input_gate.reshape(block_count, BLOCK, head_count).transpose(0, 2, 1)
    running = jnp.cumsum(forget_log_factor, axis=-1)
    totals = running[..., -1]
    to_end = totals[..., None] - running + in_gate
    block_peak = jnp.max(to_end, axis=-1)
    key_weight = jnp.exp(to_end - block_peak[..., None])
    weighted_keys = (key_float * key_weight.transpose(0, 2, 1)[..., None]).astype(jnp.bfloat16)
    block_memory = jnp.einsum(
        "bshd,bshe->bhde", weighted_keys, value_blocks, preferred_element_type=jnp.float32
    )
    empty = (
        jnp.zeros((head_count, key_width, value_width), jnp.float32),
        jnp.full((head_count,), FLOOR_LOG, jnp.float32),
        jnp.zeros((head_count,), jnp.float32),
    )
    device_state, starts = lax.scan(advance, empty, (block_memory, block_peak, totals))
    incoming = carried_in(device_state, "ep", merge_states, empty)
    memory, peak, unused = merge_states(incoming, starts)
    scores = (
        jnp.einsum("bthd,bshd->bhts", query_blocks, key_blocks, preferred_element_type=jnp.float32)
        * qk_scale
    )
    causal = jnp.tril(jnp.ones((BLOCK, BLOCK), dtype=bool))
    log_weight = running[..., :, None] - running[..., None, :] + in_gate[..., None, :]
    log_weight = jnp.where(causal, log_weight, -jnp.inf)
    carried = running + peak[..., None]
    stable = jnp.maximum(carried, jnp.max(log_weight, axis=-1))
    inner = (scores * jnp.exp(log_weight - stable[..., None])).astype(jnp.bfloat16)
    outer = jnp.exp(carried - stable)
    memory_half = memory.astype(jnp.bfloat16)
    state = outer[..., None] * jnp.einsum(
        "bthd,bhde->bhte", query_blocks, memory_half, preferred_element_type=jnp.float32
    )
    state = state + jnp.einsum(
        "bhts,bshe->bhte", inner, value_blocks, preferred_element_type=jnp.float32
    )
    state = state * lax.rsqrt(jnp.mean(state * state, axis=-1, keepdims=True) + EPSILON)
    hidden = state.transpose(0, 2, 1, 3).reshape(row_count, head_count * value_width)
    hidden = (hidden * head_norm_scale).astype(jnp.bfloat16)
    return lax.psum_scatter(
        jnp.dot(hidden, memory_output_weight, preferred_element_type=jnp.float32).astype(
            jnp.bfloat16
        ),
        "tp",
        scatter_dimension=0,
        tiled=True,
    )


def expert_half(
    second_micro_tokens,
    expert_norm_scale,
    expert_choice_index,
    group_likelihood,
    expert_raw_weight,
    gate_weight,
    up_weight,
    down_weight,
):
    token_count, model_width = second_micro_tokens.shape
    pick_count = expert_choice_index.shape[1]
    local_experts = gate_weight.shape[0]
    ep_size = lax.axis_size("ep")
    tp_size = lax.axis_size("tp")
    expert_count = local_experts * ep_size
    capacity = tp_size * max(1, 3 * pick_count * token_count // (2 * expert_count * tp_size))
    token_float = second_micro_tokens.astype(jnp.float32)
    normed = token_float * lax.rsqrt(
        jnp.mean(token_float * token_float, axis=-1, keepdims=True) + EPSILON
    )
    normed = (normed * expert_norm_scale).astype(jnp.bfloat16)
    share = expert_raw_weight / jnp.sum(expert_raw_weight, axis=1, keepdims=True)
    route_weight = group_likelihood[:, None] * share
    flat_expert = expert_choice_index.reshape(-1)
    one_hot = (flat_expert[:, None] == jnp.arange(expert_count, dtype=jnp.int32)[None, :]).astype(
        jnp.int32
    )
    slot_rank = jnp.sum(jnp.cumsum(one_hot, axis=0) * one_hot, axis=1) - 1
    owner = flat_expert // local_experts
    local_index = flat_expert % local_experts
    slot_index = owner * (local_experts * capacity) + local_index * capacity + slot_rank
    slot_total = local_experts * ep_size * capacity
    token_index = jnp.arange(token_count * pick_count, dtype=jnp.int32) // pick_count
    slot_token = jnp.zeros((slot_total,), jnp.int32).at[slot_index].set(token_index)
    slot_used = jnp.zeros((slot_total,), bool).at[slot_index].set(True)
    outgoing = jnp.where(slot_used[:, None], normed[slot_token], jnp.zeros((), jnp.bfloat16))
    outgoing = outgoing.reshape(ep_size, local_experts, capacity, model_width)
    quarter = capacity // tp_size
    own_share = lax.dynamic_slice_in_dim(outgoing, lax.axis_index("tp") * quarter, quarter, 2)
    arrived = lax.all_to_all(own_share, "ep", split_axis=0, concat_axis=0, tiled=True)
    expert_arrived = lax.all_gather(arrived, "tp", axis=2, tiled=True)
    gate = jnp.einsum(
        "serd,edf->serf", expert_arrived, gate_weight, preferred_element_type=jnp.float32
    )
    upward = jnp.einsum(
        "serd,edf->serf", expert_arrived, up_weight, preferred_element_type=jnp.float32
    )
    hidden = (jax.nn.silu(gate) * upward).astype(jnp.bfloat16)
    summed = lax.psum_scatter(
        jnp.einsum(
            "serf,efc->cser", hidden, down_weight, preferred_element_type=jnp.float32
        ).astype(jnp.bfloat16),
        "tp",
        scatter_dimension=0,
        tiled=True,
    )
    returned = lax.all_to_all(summed, "ep", split_axis=1, concat_axis=1, tiled=True)
    flat_result = returned.reshape(returned.shape[0], slot_total)
    picked = jnp.take(flat_result, slot_index, axis=1).astype(jnp.float32)
    picked = picked.reshape(flat_result.shape[0], token_count, pick_count)
    combined = jnp.sum(picked * route_weight[None], axis=2)
    return combined.T.astype(jnp.bfloat16)


def per_device(
    queries,
    keys,
    values,
    log_input_gate,
    forget_preactivation,
    forget_offset,
    head_norm_scale,
    memory_output_weight,
    second_micro_tokens,
    expert_norm_scale,
    expert_choice_index,
    group_likelihood,
    expert_raw_weight,
    gate_weight,
    up_weight,
    down_weight,
):
    mixed = recurrence_portion(
        queries,
        keys,
        values,
        log_input_gate,
        forget_preactivation,
        forget_offset,
        head_norm_scale,
        memory_output_weight,
    )
    routed = expert_half(
        second_micro_tokens,
        expert_norm_scale,
        expert_choice_index,
        group_likelihood,
        expert_raw_weight,
        gate_weight,
        up_weight,
        down_weight,
    )
    return (mixed, routed)


def solution(mesh):
    in_specs = (
        P("ep", "tp"),
        P("ep", "tp"),
        P("ep", "tp"),
        P("ep", "tp"),
        P("ep", "tp"),
        P("ep", "tp"),
        P("tp"),
        P("tp", None),
        P("ep", None),
        P(),
        P("ep", None),
        P("ep"),
        P("ep", None),
        P("ep", None, "tp"),
        P("ep", None, "tp"),
        P("ep", "tp", None),
    )
    out_specs = (P(("ep", "tp"), None), P("ep", "tp"))
    return jax.shard_map(
        per_device, mesh=mesh, in_specs=in_specs, out_specs=out_specs, check_vma=False
    )
```

profile of v0, /device:TPU:0, one launch (start us, length us, event | category | flops | bytes accessed | tf_op | source)
XLA Modules:
  0.0 474.5 jit_solution(9666437804469296286)
XLA Ops:
  8.6 3.1 fusion.13
  11.7 4.5 reduce-window.6
  16.7 4.3 scatter_custom_fusion.1
  21.1 4.5 scatter_custom_fusion
  25.7 5.8 %fusion.15 = bf16[512,4096]{1,0:T(8,128)(2,1)} fusion(bf16[512,4096]{1,0:T(8,128)(2,1)} %param.28, f32[4096]{0:T(1024)S(1)} %copy-done.6, f32[512]{0:T(512)S(1)} %add_rsqrt_fusion), kind=kLoop, calls=%fused_computation.37 | loop fusion | flops 8388608 | bytes 8407040 | tf_op jit(solution)/shard_map/convert_element_type | solution.py:131
  31.5 24.8 %gather_fusion = bf16[1536,4096]{1,0:T(8,128)(2,1)} fusion(bf16[512,4096]{1,0:T(8,128)(2,1)} %fusion.15, s32[2048]{0:T(1024)S(1)} %pad_clamp_fusion), kind=kCustom, calls=%fused_computation | custom fusion | bytes 25171968 | tf_op jit(solution)/shard_map/gather | solution.py:146
  56.3 2.8 dynamic-slice_select_fusion
  59.2 77.8 %all_to_all.10 = bf16[8,2,24,4096]{3,2,1,0:T(8,128)(2,1)S(1)} all-to-all(bf16[8,2,24,4096]{3,2,1,0:T(8,128)(2,1)S(1)} %dynamic-slice_select_fusion), channel_id=1, replica_groups=mesh['ep'=8,'tp'=4] {'ep'}, dimensions={0} | all-to-all | bytes 6291456 | tf_op jit(solution)/shard_map/all_to_all | solution.py:150
  137.0 1.9 copy.139
  142.3 1.5 fusion.44
  143.8 7.7 %while.37 = (s32[]{:T(128)}, f32[2,128,256]{2,1,0:T(8,128)S(1)}, f32[2]{0:T(128)S(1)}, f32[2]{0:T(128)S(1)}, f32[8,2,128,256]{3,2,1,0:T(8,128)}, /*index=5*/f32[...) while((s32[]{:T(128)}, f32[2,128,256]{2,1,0:T(8,128)S(1)}, ...), condition=%wide.region_3.4_spmd.clone, body=%wide.region_2.3_spmd.clone.sunk | while | flops 327699 | bytes 1311034 | solution.py:76
  152.5 67.7 %all-gather.6.cloned.1.call-done = bf16[8,2,96,4096]{3,2,0,1:T(8,128)(2,1)} async-done(((bf16[8,2,24,4096]{3,2,0,1:T(8,128)(2,1)}), bf16[8,2,96,4096]{3,2,0,1:T(8,128)(2,1)}) %all-gather.6.cloned.1.call-update) | async-done | bytes 12582928 | tf_op jit(solution)/shard_map/all_gather | solution.py:151
  220.2 7.8 %fusion.19 = f32[2,8,96,256]{3,2,1,0:T(8,128)S(1)} fusion(bf16[8,2,96,4096]{3,2,0,1:T(8,128)(2,1)} %all-gather.6.cloned.1.call-done, bf16[2,4096,256]{2,1,0:T(8,128)(2,1)} %param.33), kind=kOutput, calls=%fused_computation.42 | convolution fusion | flops 3221225472 | bytes 18350080 | tf_op jit(solution)/shard_map/serd,edf->serf/dot_general | solution.py:152
  228.0 8.7 %fusion.25 = bf16[8,2,96,256]{3,2,0,1:T(8,128)(2,1)S(1)} fusion(f32[2,8,96,256]{3,2,1,0:T(8,128)S(1)} %fusion.19, bf16[8,2,96,4096]{3,2,0,1:T(8,128)(2,1)} %all-gather.6.cloned.1.call-done, bf16[2,4096,256]{2,1,0:T(8,128)(2,1)S(1)} %copy-done.12), kind=kOutput, calls=%fused_computation.57 | convolution fusion | flops 3223584768 | bytes 19136512 | tf_op jit(solution)/shard_map/serd,edf->serf/dot_general | solution.py:155
  236.7 6.4 %convert_bitcast_fusion = bf16[4096,8,2,96]{0,3,1,2:T(8,128)(2,1)} fusion(bf16[8,2,96,256]{3,2,0,1:T(8,128)(2,1)S(1)} %fusion.25, bf16[2,256,4096]{2,1,0:T(8,128)(2,1)S(1)} %copy-done.1), kind=kOutput, calls=%fused_computation.32 | convolution fusion | flops 3227516928 | bytes 17563648 | tf_op jit(solution)/shard_map/serf,efc->cser/dot_general | solution.py:160
  245.4 22.1 %all-reduce.2 = (f32[16]{0:T(128)S(1)}, f32[16]{0:T(128)S(1)}) all-reduce(f32[16]{0:T(128)S(1)} %dynamic-update-slice, f32[16]{0:T(128)S(1)} %dynamic-update-slice.1), channel_id=2, replica_groups=mesh['ep'=8,'tp'=4] {'ep'}, use_global_device_ids=true, to_apply=%add | all-reduce | flops 32 | bytes 256
  269.4 2.7 all-gather.8.cloned.1.call-done
  272.1 8.0 %while.38 = (s32[]{:T(128)}, f32[2,128,256]{2,1,0:T(8,128)S(1)}, f32[2]{0:T(128)S(1)}, s32[]{:T(128)}, f32[8,2]{1,0:T(8,128)S(1)}, /*index=5*/f32[8,2]{1,0:T(8,1...) while((s32[]{:T(128)}, f32[2,128,256]{2,1,0:T(8,128)S(1)}, f32[2]{0:T(128)S(1)}, s32[]{:T(128)}, ...), condition=%wide.region_5.6_spmd.clone, body=%wide.region_4.5_spmd.clone.sunk | while | flops 327698 | bytes 786655 | solution.py:23
  277.8 1.1 fusion.96
  280.4 3.0 fusion.34
  283.3 4.3 fusion.23
  287.7 2.7 fusion.24
  290.4 1.2 copy.131
  291.6 1.2 copy-done.13
  292.8 7.8 %convolution_convert_fusion = bf16[1024,4096]{1,0:T(8,128)(2,1)} fusion(bf16[512,4096]{1,0:T(8,128)(2,1)S(1)} %copy-done.13, f32[64,8,8,128]{3,2,1,0:T(8,128)S(1)} %bitcast.194, f32[512]{0:T(512)S(1)} %copy-done.14), kind=kOutput, calls=%fused_computation.38 | convolution fusion | flops 4300210176 | bytes 14682112 | tf_op jit(solution)/shard_map/dot_general | solution.py:101
  300.6 69.7 %reduce-scatter.5.cloned.1.call-done = bf16[1024,8,2,96]{0,3,1,2:T(8,128)(2,1)} async-done(((bf16[4096,8,2,96]{0,3,1,2:T(8,128)(2,1)}), bf16[1024,8,2,96]{0,3,1,2:T(8,128)(2,1)}) %reduce-scatter.5.cloned.1.call-update) | async-done | bytes 3145744 | tf_op jit(solution)/shard_map/reduce_scatter | solution.py:159
  370.3 4.0 copy.140
  374.3 5.6 %all-to-all-start.1 = ((bf16[1024,8,2,96]{0,3,2,1:T(8,128)(2,1)}), bf16[1024,8,2,96]{0,3,2,1:T(8,128)(2,1)S(1)}, u32[]{:S(2)}, u32[]{:S(2)}) async-start(bf16[1024,8,2,96]{0,3,2,1:T(8,128)(2,1)} %copy.140), calls=%async_computation.3 | async-start | bytes 6291456 | tf_op jit(solution)/shard_map/all_to_all | solution.py:167
  380.7 69.8 %all-to-all-done.1 = bf16[1024,8,2,96]{0,3,2,1:T(8,128)(2,1)S(1)} async-done(((bf16[1024,8,2,96]{0,3,2,1:T(8,128)(2,1)}), bf16[1024,8,2,96]{0,3,2,1:T(8,128)(2,1)S(1)}, u32[]{:S(2)}, u32[]{:S(2)}) %all-to-all-start.1) | async-done | bytes 3145760 | tf_op jit(solution)/shard_map/all_to_all | solution.py:167
  450.4 5.4 %gather_fusion.1 = bf16[1024,1024]{1,0:T(8,128)(2,1)} fusion(bf16[1024,1536]{0,1:T(8,128)(2,1)S(1)} %bitcast.191, s32[1024]{0:T(1024)S(1)} %broadcast_clamp_fusion), kind=kCustom, calls=%fused_computation.1 | custom fusion | bytes 4198400 | tf_op jit(solution)/shard_map/jit(_take)/gather | solution.py:169
  455.8 2.7 gather.14
  458.6 9.4 %multiply_reduce_fusion = bf16[1024,512]{0,1:T(8,128)(2,1)} fusion(bf16[1024,512,2]{0,2,1:T(2,128)(2,1)S(1)} %gather.14, pred[512,2]{1,0:T(8,128)(4,1)S(1)} %copy.137, f32[512,2]{1,0:T(8,128)S(1)} %copy.141), kind=kLoop, calls=%fused_computation.44 | loop fusion | flops 3670016 | bytes 3150848 | tf_op jit(solution)/shard_map/reduce_sum | solution.py:171
  (187 shorter events, 25.0 us)
Async XLA Ops:
  7.2 213.0 %all-gather.6.cloned.1.call-start = ((), (), s32[]{:S(2)}) async-start(), calls=%async_computation.5 | async-start | bytes 15728640 | tf_op jit(solution)/shard_map/all_gather | solution.py:151
  8.6 17.1 %copy-start.6 = (f32[4096]{0:T(1024)S(1)}, f32[4096]{0:T(1024)}, u32[]{:S(2)}) copy-start(f32[4096]{0:T(1024)} %param.29) | copy-start | bytes 49156
  138.9 0.7 copy-start.9
  138.9 0.7 copy-start.10
  138.9 1.6 copy-start.5
  138.9 1.8 copy-start.2
  138.9 2.1 copy-start.3
  138.9 133.2 %all-gather.8.cloned.1.call-start = ((), (), s32[]{:S(2)}) async-start(), calls=%async_computation.7 | async-start | bytes 2359296 | tf_op jit(solution)/shard_map/all_gather | solution.py:14
  151.5 0.7 copy-start
  152.2 218.1 %reduce-scatter.5.cloned.1.call-start = ((), (), s32[]{:S(2)}) async-start(), calls=%async_computation.6 | async-start | bytes 15728640 | tf_op jit(solution)/shard_map/reduce_scatter | solution.py:159
  220.2 7.8 %copy-start.12 = (bf16[2,4096,256]{2,1,0:T(8,128)(2,1)S(1)}, bf16[2,4096,256]{2,1,0:T(8,128)(2,1)}, u32[]{:S(2)}) copy-start(bf16[2,4096,256]{2,1,0:T(8,128)(2,1)} %param.34) | copy-start | bytes 12582916
  228.0 8.7 %copy-start.1 = (bf16[2,256,4096]{2,1,0:T(8,128)(2,1)S(1)}, bf16[2,256,4096]{2,1,0:T(8,128)(2,1)}, u32[]{:S(2)}) copy-start(bf16[2,256,4096]{2,1,0:T(8,128)(2,1)} %param.35) | copy-start | bytes 12582916
  243.1 0.7 copy-start.15
  243.1 24.7 %copy-start.4 = (bf16[1024,256]{1,0:T(8,128)(2,1)S(1)}, bf16[1024,256]{1,0:T(8,128)(2,1)}, u32[]{:S(2)}) copy-start(bf16[1024,256]{1,0:T(8,128)(2,1)} %param.20) | copy-start | bytes 1572868
  243.1 224.9 %reduce-scatter.3.cloned.1.call-start = ((), (), s32[]{:S(2)}) async-start(), calls=%async_computation.4 | async-start | bytes 10485760 | tf_op jit(solution)/shard_map/reduce_scatter | solution.py:100
  287.6 4.0 copy-start.14
  290.4 2.4 copy-start.13
  374.2 6.0 %copy-start.7 = (s32[512,2]{0,1:T(2,128)S(1)}, s32[512,2]{0,1:T(2,128)}, u32[]{:S(2)}) copy-start(s32[512,2]{0,1:T(2,128)} %param.30) | copy-start | bytes 12292
  374.2 6.2 %copy-start.8 = (f32[512,2]{0,1:T(2,128)S(1)}, f32[512,2]{0,1:T(2,128)}, u32[]{:S(2)}) copy-start(f32[512,2]{0,1:T(2,128)} %param.32) | copy-start | bytes 12292
  374.3 6.2 %copy-start.11 = (f32[512]{0:T(512)S(1)}, f32[512]{0:T(512)}, u32[]{:S(2)}) copy-start(f32[512]{0:T(512)} %param.31) | copy-start | bytes 6148
  374.3 76.2 %all-to-all-start.1 = ((bf16[1024,8,2,96]{0,3,2,1:T(8,128)(2,1)}), bf16[1024,8,2,96]{0,3,2,1:T(8,128)(2,1)S(1)}, u32[]{:S(2)}, u32[]{:S(2)}) async-start(bf16[1024,8,2,96]{0,3,2,1:T(8,128)(2,1)} %copy.140), calls=%async_computation.3 | async-start | bytes 6291456 | tf_op jit(solution)/shard_map/all_to_all | solution.py:167
Sparse Core Ops, SparseCore 0:
  139.1 81.0 all-gather.5
  222.3 49.7 all-gather.7
  274.7 95.5 reduce-scatter.4
  373.3 71.3 reduce-scatter.2
where the time goes:
time: 475 us
  waiting for transfers between devices  210 us (44%)
  blocking collectives  99.9 us (21%)
  local copies, waits for them, and re-layouts  58.9 us (12%)
  other arithmetic  45.1 us (9%)
  matrix products  39.4 us (8%)
  between operations  14.9 us (3%)
  starting transfers between devices  6.03 us (1%)
    all_to_all x1, blocking collectives, expert_half(): lax.all_to_all(own_share, 'ep', split_axis=0, concat_axis=0, tiled=True)  77.8 us
    all_to_all x1, waiting for transfers between devices, expert_half(): lax.all_to_all(summed, 'ep', split_axis=1, concat_axis=1, tiled=True)  69.8 us
    reduce_scatter x1, waiting for transfers between devices, expert_half(): lax.psum_scatter(jnp.einsum('serf,efc->cser', hidden, down_weight, prefer...  69.7 us
    all_gather x1, waiting for transfers between devices, expert_half(): expert_arrived = lax.all_gather(arrived, 'tp', axis=2, tiled=True)  67.7 us
    gather x1, local copies, waits for them, and re-layouts, expert_half(): normed[slot_token]  24.8 us
    unnamed x1, blocking collectives  22.1 us
  transfers between devices with their start and end apart: 5, of which 4 were waited for; matrix products, arithmetic and copies ran while one was open for 18% of the time, Pallas kernels for 0%

commit v1 on v0

--- a/solution.py
+++ b/solution.py
@@ -164,7 +164,10 @@
         scatter_dimension=0,
         tiled=True,
     )
-    returned = lax.all_to_all(summed, "ep", split_axis=1, concat_axis=1, tiled=True)
+    returned = jnp.concatenate(
+        lax.all_to_all(jnp.stack(jnp.split(summed, lax.axis_size("ep"), axis=1)), "ep", 0, 0),
+        axis=1,
+    )
     flat_result = returned.reshape(returned.shape[0], slot_total)
     picked = jnp.take(flat_result, slot_index, axis=1).astype(jnp.float32)
     picked = picked.reshape(flat_result.shape[0], token_count, pick_count)

time: 475 us -> 486 us (1.023)
  local copies, waits for them, and re-layouts: 58.9 us -> 69.4 us
    unnamed x42 -> x49, local copies, waits for them, and re-layouts: 5.13 us -> 17.7 us
  transfers between devices with their start and end apart: 5 -> 5, of which waited for: 4 -> 4; matrix products, arithmetic and copies ran while one was open for 18% -> 20% of each run, Pallas kernels for 0% -> 0%
where the time goes in v1:
time: 486 us; the launch traced here: 485 us
  waiting for transfers between devices  210 us (43%)
  blocking collectives  99.9 us (21%)
  local copies, waits for them, and re-layouts  69.4 us (14%)
  other arithmetic  45.1 us (9%)
  matrix products  39.3 us (8%)
  between operations  14.9 us (3%)
  starting transfers between devices  5.96 us (1%)
    all_to_all x1, blocking collectives, expert_half(): lax.all_to_all(own_share, 'ep', split_axis=0, concat_axis=0, tiled=True)  77.8 us
    all_to_all x1, waiting for transfers between devices, expert_half(): lax.all_to_all(jnp.stack(jnp.split(summed, lax.axis_size('ep'), axis=1)),...  69.9 us
    reduce_scatter x1, waiting for transfers between devices, expert_half(): lax.psum_scatter(jnp.einsum('serf,efc->cser', hidden, down_weight, prefer...  69.7 us
    all_gather x1, waiting for transfers between devices, expert_half(): expert_arrived = lax.all_gather(arrived, 'tp', axis=2, tiled=True)  67.6 us
    gather x1, local copies, waits for them, and re-layouts, expert_half(): normed[slot_token]  24.8 us
    unnamed x1, blocking collectives  22.1 us
    unnamed x49, local copies, waits for them, and re-layouts  17.7 us
  transfers between devices with their start and end apart: 5, of which 4 were waited for; matrix products, arithmetic and copies ran while one was open for 20% of the time, Pallas kernels for 0%

profile of v1, /device:TPU:0, one launch (start us, length us, event | category | flops | bytes accessed | tf_op | source)
XLA Modules:
  0.0 485.0 jit_solution(6895762600064794574)
XLA Ops:
  8.6 4.5 reduce-window.6
  13.6 4.3 scatter_custom_fusion
  18.1 4.5 scatter_custom_fusion.1
  22.6 3.1 fusion.13
  25.8 5.8 %fusion.15 = bf16[512,4096]{1,0:T(8,128)(2,1)} fusion(bf16[512,4096]{1,0:T(8,128)(2,1)} %param.28, f32[4096]{0:T(1024)S(1)} %copy-done.6, f32[512]{0:T(512)S(1)} %add_rsqrt_fusion), kind=kLoop, calls=%fused_computation.37 | loop fusion | flops 8388608 | bytes 8407040 | tf_op jit(solution)/shard_map/convert_element_type | solution.py:131
  31.6 24.8 %gather_fusion = bf16[1536,4096]{1,0:T(8,128)(2,1)} fusion(bf16[512,4096]{1,0:T(8,128)(2,1)} %fusion.15, s32[2048]{0:T(1024)S(1)} %pad_clamp_fusion), kind=kCustom, calls=%fused_computation | custom fusion | bytes 25171968 | tf_op jit(solution)/shard_map/gather | solution.py:146
  56.3 2.8 dynamic-slice_select_fusion
  59.2 77.8 %all_to_all.10 = bf16[8,2,24,4096]{3,2,1,0:T(8,128)(2,1)S(1)} all-to-all(bf16[8,2,24,4096]{3,2,1,0:T(8,128)(2,1)S(1)} %dynamic-slice_select_fusion), channel_id=1, replica_groups=mesh['ep'=8,'tp'=4] {'ep'}, dimensions={0} | all-to-all | bytes 6291456 | tf_op jit(solution)/shard_map/all_to_all | solution.py:150
  137.0 1.9 copy.158
  143.8 7.8 %while.37 = (s32[]{:T(128)}, f32[2,128,256]{2,1,0:T(8,128)S(1)}, f32[2]{0:T(128)S(1)}, f32[2]{0:T(128)S(1)}, f32[8,2,128,256]{3,2,1,0:T(8,128)}, /*index=5*/f32[...) while((s32[]{:T(128)}, f32[2,128,256]{2,1,0:T(8,128)S(1)}, ...), condition=%wide.region_3.4_spmd.clone, body=%wide.region_2.3_spmd.clone.sunk | while | flops 327699 | bytes 1311534 | solution.py:76
  152.6 67.6 %all-gather.6.cloned.1.call-done = bf16[8,2,96,4096]{3,2,0,1:T(8,128)(2,1)} async-done(((bf16[8,2,24,4096]{3,2,0,1:T(8,128)(2,1)}), bf16[8,2,96,4096]{3,2,0,1:T(8,128)(2,1)}) %all-gather.6.cloned.1.call-update) | async-done | bytes 12582928 | tf_op jit(solution)/shard_map/all_gather | solution.py:151
  220.2 7.8 %fusion.19 = f32[2,8,96,256]{3,2,1,0:T(8,128)S(1)} fusion(bf16[8,2,96,4096]{3,2,0,1:T(8,128)(2,1)} %all-gather.6.cloned.1.call-done, bf16[2,4096,256]{2,1,0:T(8,128)(2,1)} %param.33), kind=kOutput, calls=%fused_computation.42 | convolution fusion | flops 3221225472 | bytes 18350080 | tf_op jit(solution)/shard_map/serd,edf->serf/dot_general | solution.py:152
  228.0 8.7 %fusion.25 = bf16[8,2,96,256]{3,2,0,1:T(8,128)(2,1)S(1)} fusion(f32[2,8,96,256]{3,2,1,0:T(8,128)S(1)} %fusion.19, bf16[8,2,96,4096]{3,2,0,1:T(8,128)(2,1)} %all-gather.6.cloned.1.call-done, bf16[2,4096,256]{2,1,0:T(8,128)(2,1)S(1)} %copy-done.12), kind=kOutput, calls=%fused_computation.57 | convolution fusion | flops 3223584768 | bytes 19136512 | tf_op jit(solution)/shard_map/serd,edf->serf/dot_general | solution.py:155
  236.7 6.4 %convert_bitcast_fusion = bf16[4096,8,2,96]{0,3,1,2:T(8,128)(2,1)} fusion(bf16[8,2,96,256]{3,2,0,1:T(8,128)(2,1)S(1)} %fusion.25, bf16[2,256,4096]{2,1,0:T(8,128)(2,1)S(1)} %copy-done.1), kind=kOutput, calls=%fused_computation.32 | convolution fusion | flops 3227516928 | bytes 17563648 | tf_op jit(solution)/shard_map/serf,efc->cser/dot_general | solution.py:160
  245.4 22.1 %all-reduce.2 = (f32[16]{0:T(128)S(1)}, f32[16]{0:T(128)S(1)}) all-reduce(f32[16]{0:T(128)S(1)} %dynamic-update-slice, f32[16]{0:T(128)S(1)} %dynamic-update-slice.1), channel_id=2, replica_groups=mesh['ep'=8,'tp'=4] {'ep'}, use_global_device_ids=true, to_apply=%add | all-reduce | flops 32 | bytes 256
  269.4 2.7 all-gather.8.cloned.1.call-done
  272.1 8.0 %while.38 = (s32[]{:T(128)}, f32[2,128,256]{2,1,0:T(8,128)S(1)}, f32[2]{0:T(128)S(1)}, s32[]{:T(128)}, f32[8,2]{1,0:T(8,128)S(1)}, /*index=5*/f32[8,2]{1,0:T(8,1...) while((s32[]{:T(128)}, f32[2,128,256]{2,1,0:T(8,128)S(1)}, f32[2]{0:T(128)S(1)}, s32[]{:T(128)}, ...), condition=%wide.region_5.6_spmd.clone, body=%wide.region_4.5_spmd.clone.sunk | while | flops 327698 | bytes 786647 | solution.py:23
  280.3 2.9 fusion.34
  283.2 4.2 fusion.23
  287.5 2.7 fusion.24
  292.7 7.8 %convolution_convert_fusion = bf16[1024,4096]{1,0:T(8,128)(2,1)} fusion(bf16[512,4096]{1,0:T(8,128)(2,1)S(1)} %copy-done.13, f32[64,8,8,128]{3,2,1,0:T(8,128)S(1)} %bitcast.242, f32[512]{0:T(512)S(1)} %copy-done.14), kind=kOutput, calls=%fused_computation.38 | convolution fusion | flops 4300210176 | bytes 14682112 | tf_op jit(solution)/shard_map/dot_general | solution.py:101
  300.5 69.7 %reduce-scatter.5.cloned.1.call-done = bf16[1024,8,2,96]{0,3,1,2:T(8,128)(2,1)} async-done(((bf16[4096,8,2,96]{0,3,1,2:T(8,128)(2,1)}), bf16[1024,8,2,96]{0,3,1,2:T(8,128)(2,1)}) %reduce-scatter.5.cloned.1.call-update) | async-done | bytes 3145744 | tf_op jit(solution)/shard_map/reduce_scatter | solution.py:159
  372.0 1.8 fusion.63
  375.5 1.8 fusion.61
  379.1 1.8 fusion.59
  380.9 1.9 fusion.58
  382.8 1.9 fusion.57
  384.7 5.6 %all-to-all-start.1 = ((bf16[8,1024,1,2,96]{1,4,3,2,0:T(8,128)(2,1)}), bf16[8,1024,1,2,96]{1,4,3,2,0:T(8,128)(2,1)S(1)}, u32[]{:S(2)}, u32[]{:S(2)}) async-start(bf16[8,1024,1,2,96]{1,4,3,2,0:T(8,128)(2,1)} %fusion.57), calls=%async_computation.3 | async-start | bytes 6291456 | tf_op jit(solution)/shard_map/all_to_all | solution.py:168
  391.0 69.9 %all-to-all-done.1 = bf16[8,1024,1,2,96]{1,4,3,2,0:T(8,128)(2,1)S(1)} async-done(((bf16[8,1024,1,2,96]{1,4,3,2,0:T(8,128)(2,1)}), bf16[8,1024,1,2,96]{1,4,3,2,0:T(8,128)(2,1)S(1)}, u32[]{:S(2)}, u32[]{:S(2)}) %all-to-all-start.1) | async-done | bytes 3145760 | tf_op jit(solution)/shard_map/all_to_all | solution.py:168
  460.9 5.4 %gather_fusion.1 = bf16[1024,1024]{1,0:T(8,128)(2,1)} fusion(bf16[1024,1536]{0,1:T(8,128)(2,1)S(1)} %bitcast.239, s32[1024]{0:T(1024)S(1)} %broadcast_clamp_fusion), kind=kCustom, calls=%fused_computation.1 | custom fusion | bytes 4198400 | tf_op jit(solution)/shard_map/jit(_take)/gather | solution.py:172
  466.2 2.7 gather.14
  469.0 9.4 %multiply_reduce_fusion = bf16[1024,512]{0,1:T(8,128)(2,1)} fusion(bf16[1024,512,2]{0,2,1:T(2,128)(2,1)S(1)} %gather.14, pred[512,2]{1,0:T(8,128)(4,1)S(1)} %copy.156, f32[512,2]{1,0:T(8,128)S(1)} %copy.166), kind=kLoop, calls=%fused_computation.44 | loop fusion | flops 3670016 | bytes 3150848 | tf_op jit(solution)/shard_map/reduce_sum | solution.py:174
  (194 shorter events, 35.3 us)
Async XLA Ops:
  7.2 18.6 %copy-start.6 = (f32[4096]{0:T(1024)S(1)}, f32[4096]{0:T(1024)}, u32[]{:S(2)}) copy-start(f32[4096]{0:T(1024)} %param.29) | copy-start | bytes 49156
  7.2 213.0 %all-gather.6.cloned.1.call-start = ((), (), s32[]{:S(2)}) async-start(), calls=%async_computation.5 | async-start | bytes 15728640 | tf_op jit(solution)/shard_map/all_gather | solution.py:151
  138.9 0.7 copy-start.9
  138.9 0.7 copy-start.10
  138.9 1.6 copy-start.5
  138.9 1.9 copy-start.3
  138.9 3.1 copy-start.2
  138.9 133.1 %all-gather.8.cloned.1.call-start = ((), (), s32[]{:S(2)}) async-start(), calls=%async_computation.7 | async-start | bytes 2359296 | tf_op jit(solution)/shard_map/all_gather | solution.py:14
  151.6 0.7 copy-start
  152.3 217.9 %reduce-scatter.5.cloned.1.call-start = ((), (), s32[]{:S(2)}) async-start(), calls=%async_computation.6 | async-start | bytes 15728640 | tf_op jit(solution)/shard_map/reduce_scatter | solution.py:159
  220.2 7.8 %copy-start.12 = (bf16[2,4096,256]{2,1,0:T(8,128)(2,1)S(1)}, bf16[2,4096,256]{2,1,0:T(8,128)(2,1)}, u32[]{:S(2)}) copy-start(bf16[2,4096,256]{2,1,0:T(8,128)(2,1)} %param.34) | copy-start | bytes 12582916
  228.0 8.7 %copy-start.1 = (bf16[2,256,4096]{2,1,0:T(8,128)(2,1)S(1)}, bf16[2,256,4096]{2,1,0:T(8,128)(2,1)}, u32[]{:S(2)}) copy-start(bf16[2,256,4096]{2,1,0:T(8,128)(2,1)} %param.35) | copy-start | bytes 12582916
  243.1 0.7 copy-start.15
  243.1 24.6 %copy-start.4 = (bf16[1024,256]{1,0:T(8,128)(2,1)S(1)}, bf16[1024,256]{1,0:T(8,128)(2,1)}, u32[]{:S(2)}) copy-start(bf16[1024,256]{1,0:T(8,128)(2,1)} %param.20) | copy-start | bytes 1572868
  243.1 235.3 %reduce-scatter.3.cloned.1.call-start = ((), (), s32[]{:S(2)}) async-start(), calls=%async_computation.4 | async-start | bytes 10485760 | tf_op jit(solution)/shard_map/reduce_scatter | solution.py:100
  287.5 4.0 copy-start.14
  290.2 2.5 copy-start.13
  384.7 5.9 %copy-start.7 = (s32[512,2]{0,1:T(2,128)S(1)}, s32[512,2]{0,1:T(2,128)}, u32[]{:S(2)}) copy-start(s32[512,2]{0,1:T(2,128)} %param.30) | copy-start | bytes 12292
  384.7 6.1 %copy-start.8 = (f32[512,2]{0,1:T(2,128)S(1)}, f32[512,2]{0,1:T(2,128)}, u32[]{:S(2)}) copy-start(f32[512,2]{0,1:T(2,128)} %param.32) | copy-start | bytes 12292
  384.7 6.2 %copy-start.11 = (f32[512]{0:T(512)S(1)}, f32[512]{0:T(512)}, u32[]{:S(2)}) copy-start(f32[512]{0:T(512)} %param.31) | copy-start | bytes 6148
  384.7 76.2 %all-to-all-start.1 = ((bf16[8,1024,1,2,96]{1,4,3,2,0:T(8,128)(2,1)}), bf16[8,1024,1,2,96]{1,4,3,2,0:T(8,128)(2,1)S(1)}, u32[]{:S(2)}, u32[]{:S(2)}) async-start(bf16[8,1024,1,2,96]{1,4,3,2,0:T(8,128)(2,1)} %fusion.57), calls=%async_computation.3 | async-start | bytes 6291456 | tf_op jit(solution)/shard_map/all_to_all | solution.py:168
Sparse Core Ops, SparseCore 0:
  139.0 81.0 all-gather.5
  222.3 49.7 all-gather.7
  274.6 95.5 reduce-scatter.4
  373.2 71.4 reduce-scatter.2
